TPU v7x, 512 devices: a whole 4x8x8 slice. The times are simulated.
512 devices in a mesh: sp: 64 (over z, y), tp: 8 (over x, core).
Axes of the slice: x: 4, y: 8, z: 8, core: 2. Of those that a mesh axis runs over, the one named last changes fastest.
Arguments:
- tokens: bfloat16 [18432, 4096], P('sp', 'tp'), may hold values from -6 to 6
- doc_ids: int32 [18432], P('sp'), may hold values from 0 to 15, never falling along the last dimension, each value on 1 to 9216 neighbouring positions
- norm_gain: float32 [2, 4096], replicated, may hold values from 0.1 to 1.9
- in_proj: bfloat16 [2, 4096, 4096], P(None, 'sp', 'tp'), may hold values from -0.09375 to 0.09375
- mix_proj: bfloat16 [2, 1024, 4096], P(None, 'sp', 'tp'), may hold values from -0.1875 to 0.1875
- out_scale: float32 [2, 4096], replicated, may hold values from 0.1 to 1.9
Outputs:
- mixed_out: bfloat16 [18432, 4096], P('sp', 'tp')
Inputs may be any that keep to these rules, and one draw needn't show every extreme that they name: `doc_ids`: document numbers never fall along the sequence, run from 0 to 15, and each document holds at most 9216 positions.
All inputs are finite; a program needn't handle non-finite values.
Results may differ from a plain program's by a relative error of at most 0.0085.
Values may be sent and summed in bfloat16 or wider, within the bound.
No kernel may reach another device: no remote copies, remote signals or barrier semaphores. Data moves between devices by JAX's collectives and lax.ppermute only.
A program may use at most 128 MiB of HBM per device.

v0:
```python
import jax
import jax.numpy as jnp
from jax import lax
from jax.sharding import PartitionSpec as P

D = 4096
WIN = 16
LAYERS = 2


epsilon = 1e-06


def laid_out(tiles, dim):
    shape = list(tiles.shape[1:])
    shape[dim] *= tiles.shape[0]
    return jnp.moveaxis(tiles, 0, dim).reshape(shape)


def gather_together(arrays, axis, dims):
    line = jnp.concatenate([a.reshape(-1) for a in arrays])
    lines, at, gathered = (lax.all_gather(line, axis), 0, [])
    for a, dim in zip(arrays, dims):
        tiles = lines[:, at : at + a.size].reshape(-1, *a.shape)
        gathered.append(laid_out(tiles, dim))
        at += a.size
    return tuple(gathered)


def from_everyone(x, axis):
    copies = jnp.broadcast_to(x, (lax.axis_size(axis), *x.shape))
    return lax.all_to_all(copies, axis, split_axis=0, concat_axis=0, tiled=True)


def gather_directly(x, axis, dim):
    tiles = from_everyone(x, axis)
    return laid_out(tiles, dim)


def from_behind(block, axis, distance):
    devices = range(lax.axis_size(axis))
    route = [(i - distance, i) for i in devices if i - distance in devices]
    return lax.ppermute(block, axis, route)


def partner_2(value, axis, stride):
    mask = 2**stride
    pairs = [(source, source ^ mask) for source in range(lax.axis_size(axis))]
    return lax.ppermute(value, axis, pairs)


def normalize(current, gain_row):
    values = current.astype(jnp.float32)
    scaled = values * lax.rsqrt(jnp.mean(values * values, axis=-1, keepdims=True) + epsilon)
    return (scaled * gain_row[None, :]).astype(jnp.bfloat16)


def pool_block(extended, ext_flags, own_flags, proj_f32, windows, local_rows):
    window_sum = jnp.zeros_like(proj_f32)
    window_count = jnp.zeros_like(proj_f32)
    for offset in range(WIN):
        begin = WIN - 1 - offset
        shifted = extended[begin : begin + local_rows]
        same_doc = ext_flags[begin : begin + local_rows] == own_flags
        taken = same_doc[:, None] & (offset < windows)[None, :]
        window_sum = window_sum + jnp.where(taken, shifted, jnp.float32(0.0))
        window_count = window_count + taken.astype(jnp.float32)
    return (window_sum / window_count - proj_f32).astype(jnp.bfloat16)


def shards(tokens, doc_ids, norm_gain, in_proj, mix_proj, out_scale):
    local_rows = tokens.shape[0]
    local_width = tokens.shape[1]
    block_width = D // 8
    tp_count = lax.axis_size("tp")
    half_bit = tp_count.bit_length() - 2
    tp_index = lax.axis_index("tp")
    chan_start = tp_index * local_width
    channels = chan_start + jnp.arange(local_width, dtype=jnp.int32)
    windows = jnp.left_shift(jnp.int32(2), channels // block_width % 4)
    low_side = tp_index < tp_count // 2
    doc_flags = (doc_ids + 1).astype(jnp.bfloat16)
    in_whole, mix_whole = gather_together((in_proj, mix_proj), "sp", (1, 1))
    current = tokens
    for depth_idx in range(LAYERS):
        gathered = gather_directly(current, "tp", 1)
        normed = normalize(gathered, norm_gain[depth_idx])
        proj_sum = jnp.dot(normed, in_whole[depth_idx], preferred_element_type=jnp.float32)
        projected = proj_sum.astype(jnp.bfloat16)
        tail_rows, tail_flags = from_behind(
            (projected[local_rows - (WIN - 1) :], doc_flags[local_rows - (WIN - 1) :]), "sp", 1
        )
        extended = jnp.concatenate([tail_rows, projected], axis=0).astype(jnp.float32)
        ext_flags = jnp.concatenate([tail_flags, doc_flags], axis=0)
        pooled = pool_block(
            extended, ext_flags, doc_flags, projected.astype(jnp.float32), windows, local_rows
        )
        partner = partner_2(pooled, "tp", half_bit)
        low_part = jnp.where(low_side, pooled, partner)
        high_part = jnp.where(low_side, partner, pooled)
        group_inputs = jnp.concatenate([low_part, high_part], axis=1)
        pieces_out = jnp.dot(group_inputs, mix_whole[depth_idx], preferred_element_type=jnp.float32)
        scale_row = lax.dynamic_slice_in_dim(out_scale[depth_idx], chan_start, local_width, 0)
        current = (pieces_out * scale_row[None, :]).astype(jnp.bfloat16)
    return current


def solution(mesh):
    placed = (P("sp", "tp"), P("sp"), P(), P(None, "sp", "tp"), P(None, "sp", "tp"), P())
    return jax.shard_map(
        shards, mesh=mesh, in_specs=placed, out_specs=P("sp", "tp"), check_vma=False
    )
```

profile of v0, /device:TPU:256, one launch (start us, length us, event | category | flops | bytes accessed | tf_op | source)
XLA Modules:
  0.0 250.4 jit_solution(2940529422567434063)
XLA Ops:
  9.8 3.5 %collective-permute-start.1 = (bf16[15]{0:T(256)(128)(2,1)S(1)}, bf16[15]{0:T(256)(128)(2,1)S(1)}, u32[]{:S(2)}, u32[]{:S(2)}) collective-permute-start(bf16[15]{0:T(256)(128)(2,1)S(1)} %slice.205), channel_id=1, source_target_pairs={{0,8},{8,16},{16,24},{24,32},{32,40},{40,48},{48,56},{56,64},{64,7... | collective-permute-start | bytes 98 | tf_op jit(solution)/shard_map/ppermute | solution.py:43
  13.2 2.7 %broadcast_in_dim.39 = bf16[8,288,512]{2,1,0:T(8,128)(2,1)} broadcast(bf16[288,512]{1,0:T(8,128)(2,1)} %param.6), dimensions={1,2} | broadcast | bytes 2654208 | tf_op jit(solution)/shard_map/broadcast_in_dim | solution.py:31
  15.9 4.3 %all-to-all-start = ((bf16[8,288,512]{2,1,0:T(8,128)(2,1)}), bf16[8,288,512]{2,1,0:T(8,128)(2,1)S(1)}, u32[]{:S(2)}, u32[]{:S(2)}) async-start(bf16[8,288,512]{2,1,0:T(8,128)(2,1)} %broadcast_in_dim.39), calls=%async_computation | async-start | bytes 4718592 | tf_op jit(solution)/shard_map/all_to_all | solution.py:32
  20.7 29.4 %all-to-all-done = bf16[8,288,512]{2,1,0:T(8,128)(2,1)S(1)} async-done(((bf16[8,288,512]{2,1,0:T(8,128)(2,1)}), bf16[8,288,512]{2,1,0:T(8,128)(2,1)S(1)}, u32[]{:S(2)}, u32[]{:S(2)}) %all-to-all-start) | async-done | bytes 2359328 | tf_op jit(solution)/shard_map/all_to_all | solution.py:32
  51.7 68.5 %all-gather.3.cloned.1.call-done = bf16[5242880]{0:T(1024)(128)(2,1)} async-done(((bf16[81920]{0:T(1024)(128)(2,1)}), bf16[5242880]{0:T(1024)(128)(2,1)}) %all-gather.3.cloned.1.call-update) | async-done | bytes 10485776 | tf_op jit(solution)/shard_map/all_gather | solution.py:22
  120.1 12.0 %reshape.163 = bf16[64,81920]{1,0:T(8,128)(2,1)} reshape(bf16[5242880]{0:T(1024)(128)(2,1)} %all-gather.3.cloned.1.call-done) | data formatting | bytes 20971520 | tf_op jit(solution)/shard_map/all_gather | solution.py:22
  132.1 7.2 %slice.260 = bf16[64,65536]{1,0:T(8,128)(2,1)} slice(bf16[64,81920]{1,0:T(8,128)(2,1)} %reshape.163), slice={[0:64], [0:65536]} | slice | bytes 16777216 | tf_op jit(solution)/shard_map/slice | solution.py:24
  139.3 9.9 %copy.13 = bf16[8,8,128,512]{3,2,1,0:T(8,128)(2,1)} copy(bf16[8,8,128,512]{3,1,2,0:T(8,128)(2,1)} %bitcast.36) | data formatting | bytes 16777216
  149.2 5.2 %fusion.71 = (bf16[1,64,64,512]{3,2,0,1:T(8,128)(2,1)}, bf16[1,64,64,512]{3,2,0,1:T(8,128)(2,1)S(1)}) fusion(bf16[2,64,64,512]{3,2,0,1:T(8,128)(2,1)} %bitcast.35), kind=kLoop, calls=%fused_computation.184 | loop fusion | bytes 16777216 | tf_op jit(solution)/shard_map/slice | solution.py:88
  154.5 1.4 convolution_convert_fusion.1
  155.9 2.2 collective-permute-start
  159.0 6.0 %collective-permute-done = bf16[15,512]{1,0:T(8,128)(2,1)S(1)} collective-permute-done((bf16[15,512]{1,0:T(8,128)(2,1)S(1)}, bf16[15,512]{1,0:T(8,128)(2,1)S(1)}, u32[]{:S(2)}, u32[]{:S(2)}) %collective-permute-start) | collective-permute-done | bytes 15392 | tf_op jit(solution)/shard_map/ppermute | solution.py:43
  165.2 2.9 %subtract_convert_fusion.1 = bf16[288,512]{1,0:T(8,128)(2,1)S(1)} fusion(bf16[288,512]{1,0:T(8,128)(2,1)S(1)} %convolution_convert_fusion.1, f32[303,512]{1,0:T(8,128)S(1)} %maximum_convert_fusion, pred[512]{0:T(512)(128)(4,1)S(1)} %get-tuple-element.34, pred[512]{0:T(512)(128)(4,1)S(1)} %get-tuple-element.35, pred[512]{0:T(512)(128)(4,1)S(1)} %get-tuple-element.36, ...), kind=kLoop, calls=%fused_computation.120 | loop fusion | flops 12091392 | bytes 10039808 | tf_op jit(solution)/shard_map/convert_element_type | solution.py:68
  168.1 4.9 %collective-permute-start.2 = (bf16[288,512]{1,0:T(8,128)(2,1)S(1)}, bf16[288,512]{1,0:T(8,128)(2,1)S(1)}, u32[]{:S(2)}, u32[]{:S(2)}) collective-permute-start(bf16[288,512]{1,0:T(8,128)(2,1)S(1)} %subtract_convert_fusion.1), channel_id=1, source_target_pairs={{0,4},{1,5},{2,6},{3,7},{4,0},{5,1},{6,2},{7,3},{8,12},{9,13},{10,... | collective-permute-start | bytes 884744 | tf_op jit(solution)/shard_map/ppermute | solution.py:49
  173.2 5.7 %collective-permute-done.2 = bf16[288,512]{1,0:T(8,128)(2,1)S(1)} collective-permute-done((bf16[288,512]{1,0:T(8,128)(2,1)S(1)}, bf16[288,512]{1,0:T(8,128)(2,1)S(1)}, u32[]{:S(2)}, u32[]{:S(2)}) %collective-permute-start.2) | collective-permute-done | bytes 294944 | tf_op jit(solution)/shard_map/ppermute | solution.py:49
  179.5 1.6 broadcast_in_dim.41
  181.1 4.3 %all-to-all-start.1 = ((bf16[8,288,512]{2,1,0:T(8,128)(2,1)}), bf16[8,288,512]{2,1,0:T(8,128)(2,1)S(1)}, u32[]{:S(2)}, u32[]{:S(2)}) async-start(bf16[8,288,512]{2,1,0:T(8,128)(2,1)} %broadcast_in_dim.41), calls=%async_computation.1 | async-start | bytes 4718592 | tf_op jit(solution)/shard_map/all_to_all | solution.py:32
  185.3 30.0 %all-to-all-done.1 = bf16[8,288,512]{2,1,0:T(8,128)(2,1)S(1)} async-done(((bf16[8,288,512]{2,1,0:T(8,128)(2,1)}), bf16[8,288,512]{2,1,0:T(8,128)(2,1)S(1)}, u32[]{:S(2)}, u32[]{:S(2)}) %all-to-all-start.1) | async-done | bytes 2359328 | tf_op jit(solution)/shard_map/all_to_all | solution.py:32
  218.1 1.4 convolution_convert_fusion
  219.5 1.9 collective-permute-start.3
  221.4 7.0 %collective-permute-done.3 = bf16[15,512]{1,0:T(8,128)(2,1)S(1)} collective-permute-done((bf16[15,512]{1,0:T(8,128)(2,1)S(1)}, bf16[15,512]{1,0:T(8,128)(2,1)S(1)}, u32[]{:S(2)}, u32[]{:S(2)}) %collective-permute-start.3) | collective-permute-done | bytes 15392 | tf_op jit(solution)/shard_map/ppermute | solution.py:43
  228.6 2.9 %subtract_convert_fusion = bf16[288,512]{1,0:T(8,128)(2,1)S(1)} fusion(bf16[288,512]{1,0:T(8,128)(2,1)S(1)} %convolution_convert_fusion, f32[303,512]{1,0:T(8,128)S(1)} %maximum_convert_fusion.1, pred[512]{0:T(512)(128)(4,1)S(1)} %copy-done.12, pred[512]{0:T(512)(128)(4,1)S(1)} %copy-done.14, pred[512]{0:T(512)(128)(4,1)S(1)} %copy-done.4, ...), kind=kLoop, calls=%fused_computation.119 | loop fusion | flops 12091392 | bytes 10039808 | tf_op jit(solution)/shard_map/convert_element_type | solution.py:68
  231.6 2.3 collective-permute-start.4
  233.9 8.4 %collective-permute-done.4 = bf16[288,512]{1,0:T(8,128)(2,1)S(1)} collective-permute-done((bf16[288,512]{1,0:T(8,128)(2,1)S(1)}, bf16[288,512]{1,0:T(8,128)(2,1)S(1)}, u32[]{:S(2)}, u32[]{:S(2)}) %collective-permute-start.4) | collective-permute-done | bytes 294944 | tf_op jit(solution)/shard_map/ppermute | solution.py:49
  (82 shorter events, 10.8 us)
Async XLA Ops:
  6.5 13.7 %copy-start.1 = (f32[2,4096]{1,0:T(2,128)S(1)}, f32[2,4096]{1,0:T(2,128)}, u32[]{:S(2)}) copy-start(f32[2,4096]{1,0:T(2,128)} %param.8) | copy-start | bytes 98308
  6.5 14.0 %copy-start.2 = (f32[2,4096]{1,0:T(2,128)S(1)}, f32[2,4096]{1,0:T(2,128)}, u32[]{:S(2)}) copy-start(f32[2,4096]{1,0:T(2,128)} %param.11) | copy-start | bytes 98308
  6.5 113.6 %all-gather.3.cloned.1.call-start = ((), (), s32[]{:S(2)}) async-start(), calls=%async_computation.2 | async-start | bytes 10649600 | tf_op jit(solution)/shard_map/all_gather | solution.py:22
  9.8 10.9 %collective-permute-start.1 = (bf16[15]{0:T(256)(128)(2,1)S(1)}, bf16[15]{0:T(256)(128)(2,1)S(1)}, u32[]{:S(2)}, u32[]{:S(2)}) collective-permute-start(bf16[15]{0:T(256)(128)(2,1)S(1)} %slice.205), channel_id=1, source_target_pairs={{0,8},{8,16},{16,24},{24,32},{32,40},{40,48},{48,56},{56,64},{64,7... | collective-permute-start | bytes 98 | tf_op jit(solution)/shard_map/ppermute | solution.py:43
  15.9 34.3 %all-to-all-start = ((bf16[8,288,512]{2,1,0:T(8,128)(2,1)}), bf16[8,288,512]{2,1,0:T(8,128)(2,1)S(1)}, u32[]{:S(2)}, u32[]{:S(2)}) async-start(bf16[8,288,512]{2,1,0:T(8,128)(2,1)} %broadcast_in_dim.39), calls=%async_computation | async-start | bytes 4718592 | tf_op jit(solution)/shard_map/all_to_all | solution.py:32
  20.4 144.7 %copy-start.3 = (pred[512]{0:T(512)(128)(4,1)}, pred[512]{0:T(512)(128)(4,1)S(1)}, u32[]{:S(2)}) copy-start(pred[512]{0:T(512)(128)(4,1)S(1)} %get-tuple-element.36) | copy-start | bytes 1540
  20.4 144.7 %copy-start.5 = (pred[512]{0:T(512)(128)(4,1)}, pred[512]{0:T(512)(128)(4,1)S(1)}, u32[]{:S(2)}) copy-start(pred[512]{0:T(512)(128)(4,1)S(1)} %get-tuple-element.37) | copy-start | bytes 1540
  20.5 144.6 %copy-start.7 = (pred[512]{0:T(512)(128)(4,1)}, pred[512]{0:T(512)(128)(4,1)S(1)}, u32[]{:S(2)}) copy-start(pred[512]{0:T(512)(128)(4,1)S(1)} %get-tuple-element.48) | copy-start | bytes 1540
  20.5 144.6 %copy-start.9 = (pred[512]{0:T(512)(128)(4,1)}, pred[512]{0:T(512)(128)(4,1)S(1)}, u32[]{:S(2)}) copy-start(pred[512]{0:T(512)(128)(4,1)S(1)} %get-tuple-element.49) | copy-start | bytes 1540
  20.5 144.6 %copy-start.11 = (pred[512]{0:T(512)(128)(4,1)}, pred[512]{0:T(512)(128)(4,1)S(1)}, u32[]{:S(2)}) copy-start(pred[512]{0:T(512)(128)(4,1)S(1)} %get-tuple-element.34) | copy-start | bytes 1540
  20.5 144.6 %copy-start.13 = (pred[512]{0:T(512)(128)(4,1)}, pred[512]{0:T(512)(128)(4,1)S(1)}, u32[]{:S(2)}) copy-start(pred[512]{0:T(512)(128)(4,1)S(1)} %get-tuple-element.35) | copy-start | bytes 1540
  20.6 144.6 %copy-start.15 = (pred[512]{0:T(512)(128)(4,1)}, pred[512]{0:T(512)(128)(4,1)S(1)}, u32[]{:S(2)}) copy-start(pred[512]{0:T(512)(128)(4,1)S(1)} %get-tuple-element.44) | copy-start | bytes 1540
  20.6 144.6 %copy-start.17 = (pred[512]{0:T(512)(128)(4,1)}, pred[512]{0:T(512)(128)(4,1)S(1)}, u32[]{:S(2)}) copy-start(pred[512]{0:T(512)(128)(4,1)S(1)} %get-tuple-element.45) | copy-start | bytes 1540
  155.9 9.1 %collective-permute-start = (bf16[15,512]{1,0:T(8,128)(2,1)S(1)}, bf16[15,512]{1,0:T(8,128)(2,1)S(1)}, u32[]{:S(2)}, u32[]{:S(2)}) collective-permute-start(bf16[15,512]{1,0:T(8,128)(2,1)S(1)} %slice.262), channel_id=1, source_target_pairs={{0,8},{8,16},{16,24},{24,32},{32,40},{40,48},{48,56},{56,64},{64,7... | collective-permute-start | bytes 46088 | tf_op jit(solution)/shard_map/ppermute | solution.py:43
  168.1 10.8 %collective-permute-start.2 = (bf16[288,512]{1,0:T(8,128)(2,1)S(1)}, bf16[288,512]{1,0:T(8,128)(2,1)S(1)}, u32[]{:S(2)}, u32[]{:S(2)}) collective-permute-start(bf16[288,512]{1,0:T(8,128)(2,1)S(1)} %subtract_convert_fusion.1), channel_id=1, source_target_pairs={{0,4},{1,5},{2,6},{3,7},{4,0},{5,1},{6,2},{7,3},{8,12},{9,13},{10,... | collective-permute-start | bytes 884744 | tf_op jit(solution)/shard_map/ppermute | solution.py:49
  181.1 34.2 %all-to-all-start.1 = ((bf16[8,288,512]{2,1,0:T(8,128)(2,1)}), bf16[8,288,512]{2,1,0:T(8,128)(2,1)S(1)}, u32[]{:S(2)}, u32[]{:S(2)}) async-start(bf16[8,288,512]{2,1,0:T(8,128)(2,1)} %broadcast_in_dim.41), calls=%async_computation.1 | async-start | bytes 4718592 | tf_op jit(solution)/shard_map/all_to_all | solution.py:32
  218.1 10.5 %copy-start.8 = (pred[512]{0:T(512)(128)(4,1)S(1)}, pred[512]{0:T(512)(128)(4,1)}, u32[]{:S(2)}) copy-start(pred[512]{0:T(512)(128)(4,1)} %copy-done.7) | copy-start | bytes 1540
  218.1 10.5 %copy-start.10 = (pred[512]{0:T(512)(128)(4,1)S(1)}, pred[512]{0:T(512)(128)(4,1)}, u32[]{:S(2)}) copy-start(pred[512]{0:T(512)(128)(4,1)} %copy-done.9) | copy-start | bytes 1540
  218.1 10.5 %copy-start.12 = (pred[512]{0:T(512)(128)(4,1)S(1)}, pred[512]{0:T(512)(128)(4,1)}, u32[]{:S(2)}) copy-start(pred[512]{0:T(512)(128)(4,1)} %copy-done.11) | copy-start | bytes 1540
  218.1 10.5 %copy-start.14 = (pred[512]{0:T(512)(128)(4,1)S(1)}, pred[512]{0:T(512)(128)(4,1)}, u32[]{:S(2)}) copy-start(pred[512]{0:T(512)(128)(4,1)} %copy-done.13) | copy-start | bytes 1540
  218.1 10.5 %copy-start.16 = (pred[512]{0:T(512)(128)(4,1)S(1)}, pred[512]{0:T(512)(128)(4,1)}, u32[]{:S(2)}) copy-start(pred[512]{0:T(512)(128)(4,1)} %copy-done.15) | copy-start | bytes 1540
  218.1 10.5 %copy-start.18 = (pred[512]{0:T(512)(128)(4,1)S(1)}, pred[512]{0:T(512)(128)(4,1)}, u32[]{:S(2)}) copy-start(pred[512]{0:T(512)(128)(4,1)} %copy-done.17) | copy-start | bytes 1540
  219.5 9.0 %collective-permute-start.3 = (bf16[15,512]{1,0:T(8,128)(2,1)S(1)}, bf16[15,512]{1,0:T(8,128)(2,1)S(1)}, u32[]{:S(2)}, u32[]{:S(2)}) collective-permute-start(bf16[15,512]{1,0:T(8,128)(2,1)S(1)} %slice.282), channel_id=1, source_target_pairs={{0,8},{8,16},{16,24},{24,32},{32,40},{40,48},{48,56},{56,64},{64,7... | collective-permute-start | bytes 46088 | tf_op jit(solution)/shard_map/ppermute | solution.py:43
  231.6 10.7 %collective-permute-start.4 = (bf16[288,512]{1,0:T(8,128)(2,1)S(1)}, bf16[288,512]{1,0:T(8,128)(2,1)S(1)}, u32[]{:S(2)}, u32[]{:S(2)}) collective-permute-start(bf16[288,512]{1,0:T(8,128)(2,1)S(1)} %subtract_convert_fusion), channel_id=1, source_target_pairs={{0,4},{1,5},{2,6},{3,7},{4,0},{5,1},{6,2},{7,3},{8,12},{9,13},{10,... | collective-permute-start | bytes 884744 | tf_op jit(solution)/shard_map/ppermute | solution.py:49
  (4 other events, 25.5 us)
Sparse Core Ops, SparseCore 0:
  10.3 109.7 all-gather.2
where the time goes:
time: 251 us; the launch traced here: 250 us
  waiting for transfers between devices  155 us (62%)
  local copies, waits for them, and re-layouts  43.4 us (17%)
  starting transfers between devices  23.3 us (9%)
  between operations  13.9 us (6%)
  other arithmetic  10.2 us (4%)
  matrix products  4.45 us (2%)
    all_gather x1, waiting for transfers between devices, gather_together(): lines, at, gathered = (lax.all_gather(line, axis), 0, [])  68.5 us
    all_to_all x2, waiting for transfers between devices, from_everyone(): return lax.all_to_all(copies, axis, split_axis=0, concat_axis=0, tiled=True)  59.4 us
    ppermute x2, waiting for transfers between devices, partner_2(): return lax.ppermute(value, axis, pairs)  14.1 us
    unnamed x42, local copies, waits for them, and re-layouts  13.7 us
    ppermute x3, waiting for transfers between devices, from_behind(): return lax.ppermute(block, axis, route)  13 us
    all_gather x1, local copies, waits for them, and re-layouts, gather_together(): lines, at, gathered = (lax.all_gather(line, axis), 0, [])  12 us
    all_to_all x2, starting transfers between devices, from_everyone(): return lax.all_to_all(copies, axis, split_axis=0, concat_axis=0, tiled=True)  8.55 us
    ppermute x3, starting transfers between devices, from_behind(): return lax.ppermute(block, axis, route)  7.58 us
  transfers between devices with their start and end apart: 8, of which 7 were waited for; matrix products, arithmetic and copies ran while one was open for 3% of the time, Pallas kernels for 0%

commit v1 on v0

v1 whole, which is shorter than its diff:
```python
import jax
import jax.numpy as jnp
from jax import lax
from jax.experimental import pallas as pl
from jax.experimental.pallas import tpu as pltpu
from jax.sharding import PartitionSpec as P

D = 4096
WIN = 16
BLOCK = 512
SIDE = 8
IN_ROWS = 64
MIX_ROWS = 16
HALF = 256
EPS = 1e-06

VMEM = pltpu.VMEM
ANY = pl.ANY


def flat_perm(fn):
    pairs = []
    for z in range(SIDE):
        for y in range(SIDE):
            to_z, to_y = fn(z, y)
            pairs.append((z * SIDE + y, (to_z % SIDE) * SIDE + to_y % SIDE))
    return pairs


def y_groups():
    return [[z * SIDE + y for y in range(SIDE)] for z in range(SIDE)]


def z_groups():
    return [[z * SIDE + y for z in range(SIDE)] for y in range(SIDE)]


def spread(x, axis, groups, count):
    copies = jnp.broadcast_to(x, (count, *x.shape))
    return lax.all_to_all(copies, axis, split_axis=0, concat_axis=0, tiled=True, axis_index_groups=groups)


def weight_copies(sources, kind, lo, rows, dest, sems):
    if kind == "whole":
        src = sources[0]
        return [pltpu.make_async_copy(src.at[:, :, pl.ds(lo, rows), :], dest, sems.at[0])]
    first, second = sources
    return [
        pltpu.make_async_copy(
            first.at[:, :, pl.ds(lo, rows), :], dest.at[:, :, :, pl.ds(0, HALF)], sems.at[0]
        )
    ] + [
        pltpu.make_async_copy(
            second.at[y, :, pl.ds(lo, rows), :], dest.at[:, y, :, pl.ds(HALF, HALF)], sems.at[1 + y]
        )
        for y in range(SIDE)
    ]


def project_pool(pieces, order, gain, meta, weights, kind):
    n_x = len(pieces)
    n_w = len(weights)
    rows = pieces[0].shape[1]

    def kernel(*refs):
        order_ref = refs[0]
        x_refs = refs[1 : 1 + n_x]
        gain_ref, meta_ref = refs[1 + n_x : 3 + n_x]
        w_refs = refs[3 + n_x : 3 + n_x + n_w]
        out_ref, w_all, acc, scale, sems = refs[3 + n_x + n_w :]
        copies = weight_copies(w_refs, kind, 0, IN_ROWS, w_all, sems)
        for c in copies:
            c.start()
        total = jnp.zeros((rows, BLOCK), jnp.float32)
        for x_ref in x_refs:
            def add_square(i, total, x_ref=x_ref):
                v = x_ref[i].astype(jnp.float32)
                return total + v * v
            total = lax.fori_loop(0, x_ref.shape[0], add_square, total)
        mean = jnp.sum(total, axis=1, keepdims=True) * (1.0 / D)
        scale[...] = jnp.broadcast_to(lax.rsqrt(mean + EPS), (rows, 128))
        acc[...] = jnp.zeros_like(acc)
        for c in copies:
            c.wait()
        at = 0
        for x_ref in x_refs:
            def step(i, carry, x_ref=x_ref, at=at):
                block = order_ref[at + i]
                v = x_ref[i].astype(jnp.float32)
                normed = v * scale[:, 0:1] * gain_ref[pl.ds(block, 1), :]
                w = w_all[block].reshape(BLOCK, BLOCK)
                acc[...] += jnp.dot(normed.astype(jnp.bfloat16), w, preferred_element_type=jnp.float32)
                return carry
            lax.fori_loop(0, x_ref.shape[0], step, 0)
            at += x_ref.shape[0]
        for c in range(BLOCK // 128):
            lanes = pl.ds(c * 128, 128)
            proj = acc[:, lanes].astype(jnp.bfloat16).astype(jnp.float32)
            total = proj
            for j in range(4):
                moved = pltpu.roll(total, 2**j, 0)
                total = total + jnp.where(meta_ref[j] > 0.0, moved, 0.0)
            pooled = total * meta_ref[4] - proj
            out_ref[:, lanes] = pooled[WIN:].astype(jnp.bfloat16)

    n_sems = 1 if kind == "whole" else 1 + SIDE
    return pl.pallas_call(
        kernel,
        out_shape=jax.ShapeDtypeStruct((rows - WIN, BLOCK), jnp.bfloat16),
        in_specs=[pl.BlockSpec(memory_space=pltpu.SMEM)]
        + [pl.BlockSpec(memory_space=VMEM)] * (n_x + 2)
        + [pl.BlockSpec(memory_space=ANY)] * n_w,
        out_specs=pl.BlockSpec(memory_space=VMEM),
        scratch_shapes=[
            VMEM((SIDE, SIDE, IN_ROWS, BLOCK), jnp.bfloat16),
            VMEM((rows, BLOCK), jnp.float32),
            VMEM((rows, 128), jnp.float32),
            pltpu.SemaphoreType.DMA((n_sems,)),
        ],
        compiler_params=pltpu.CompilerParams(vmem_limit_bytes=40 * 1024 * 1024),
        cost_estimate=pl.CostEstimate(
            flops=2 * rows * D * BLOCK, bytes_accessed=7 * 1024 * 1024, transcendentals=0
        ),
        name="project_pool",
    )(order, *pieces, gain, meta, *weights)


def mix(side, own, other, scale_row, weights, kind):
    n_w = len(weights)
    rows = own.shape[0]

    def kernel(*refs):
        side_ref, own_ref, other_ref, scale_ref = refs[:4]
        w_refs = refs[4 : 4 + n_w]
        out_ref, w_all, sems = refs[4 + n_w :]
        copies = weight_copies(w_refs, kind, IN_ROWS, MIX_ROWS, w_all, sems)
        for c in copies:
            c.start()
        for c in copies:
            c.wait()
        mine = side_ref[0] * (SIDE // 2)
        theirs = (1 - side_ref[0]) * (SIDE // 2)
        w_own = w_all[pl.ds(mine, SIDE // 2)].reshape(BLOCK, BLOCK)
        w_other = w_all[pl.ds(theirs, SIDE // 2)].reshape(BLOCK, BLOCK)
        total = jnp.dot(own_ref[...], w_own, preferred_element_type=jnp.float32)
        total = total + jnp.dot(other_ref[...], w_other, preferred_element_type=jnp.float32)
        out_ref[...] = (total * scale_ref[...]).astype(jnp.bfloat16)

    n_sems = 1 if kind == "whole" else 1 + SIDE
    return pl.pallas_call(
        kernel,
        out_shape=jax.ShapeDtypeStruct((rows, BLOCK), jnp.bfloat16),
        in_specs=[pl.BlockSpec(memory_space=pltpu.SMEM)]
        + [pl.BlockSpec(memory_space=VMEM)] * 3
        + [pl.BlockSpec(memory_space=ANY)] * n_w,
        out_specs=pl.BlockSpec(memory_space=VMEM),
        scratch_shapes=[
            VMEM((SIDE, SIDE, MIX_ROWS, BLOCK), jnp.bfloat16),
            pltpu.SemaphoreType.DMA((n_sems,)),
        ],
        compiler_params=pltpu.CompilerParams(vmem_limit_bytes=24 * 1024 * 1024),
        cost_estimate=pl.CostEstimate(
            flops=4 * rows * BLOCK * BLOCK, bytes_accessed=2 * 1024 * 1024, transcendentals=0
        ),
        name="mix",
    )(side, own, other, scale_row, *weights)


def tp_perm(fn):
    return [(t, fn(t) % 8) for t in range(8)]


def shards(tokens, doc_ids, norm_gain, in_proj, mix_proj, out_scale):
    rows = tokens.shape[0]
    tp = lax.axis_index("tp")
    sp = lax.axis_index("sp")
    first = sp == 0
    per_layer = jnp.concatenate([in_proj, mix_proj], axis=1)

    w1 = lax.all_gather(per_layer[1], "sp", axis=0, tiled=True)
    w1 = w1.reshape(SIDE, SIDE, IN_ROWS + MIX_ROWS, BLOCK)

    both = IN_ROWS + MIX_ROWS
    left = spread(per_layer[0, :, :HALF], "sp", y_groups(), SIDE)
    right = spread(per_layer[0, :, HALF:], "sp", z_groups(), SIDE)
    left = spread(left.reshape(SIDE * both, HALF), "sp", z_groups(), SIDE)
    right = spread(right.reshape(SIDE * both, HALF), "sp", y_groups(), SIDE)
    left = left.reshape(SIDE, SIDE, both, HALF)
    right = right.reshape(SIDE, SIDE, both, HALF)

    halo = 2 * WIN
    flags = (doc_ids + 1).astype(jnp.bfloat16)
    flag_row = jnp.pad(flags[rows - halo :], (0, BLOCK - halo)).reshape(1, BLOCK)
    tail = jnp.concatenate([tokens[rows - halo :], jnp.pad(flag_row, ((0, 15), (0, 0)))], axis=0)
    route = [(i, i + 1) for i in range(SIDE * SIDE - 1)]
    tail = lax.ppermute(tail, "sp", route)
    ext_tokens = jnp.concatenate([tail[:halo], tokens], axis=0)
    ext_docs = jnp.concatenate([tail[halo, :halo], flags], axis=0).astype(jnp.float32)

    window = jnp.left_shift(jnp.int32(2), tp % 4)
    masks, run = [], jnp.ones_like(ext_docs)
    for offset in range(1, WIN):
        same = jnp.pad(ext_docs[:-offset], (offset, 0)) == ext_docs
        same = same & (offset < window)
        run = run + same.astype(jnp.float32)
        if offset in (1, 2, 4, 8):
            masks.append(same.astype(jnp.float32))
    meta = jnp.stack(masks + [1.0 / run], axis=0)
    meta = jnp.broadcast_to(meta[:, :, None], (5, rows + halo, 128))

    side = (tp // 4).reshape(1).astype(jnp.int32)
    gain = norm_gain.reshape(2, 8, BLOCK)
    scale = lax.dynamic_slice(out_scale, (0, tp * BLOCK), (2, BLOCK))
    partner = tp_perm(lambda t: t ^ 4)

    gathered = spread(ext_tokens, "tp", None, 8)
    pooled = project_pool(
        [gathered], jnp.arange(8, dtype=jnp.int32), gain[0], meta, [left, right], "halves"
    )
    other = lax.ppermute(pooled, "tp", partner)
    current = mix(side, pooled, other, scale[0:1], [left, right], "halves")

    arrived = [current] + [lax.ppermute(current, "tp", tp_perm(lambda t, k=k: t - 2 * k)) for k in (1, 2, 3)]
    mine = jnp.stack(arrived, axis=0)
    theirs = lax.ppermute(mine, "tp", tp_perm(lambda t: t ^ 1))
    hops = (jnp.arange(4, dtype=jnp.int32) + tp // 2) % 4
    order = jnp.concatenate([2 * hops + tp % 2, 2 * hops + 1 - tp % 2])
    pooled = project_pool([mine, theirs], order, gain[1], meta[:, WIN:], [w1], "whole")
    other = lax.ppermute(pooled, "tp", partner)
    return mix(side, pooled, other, scale[1:2], [w1], "whole")


def solution(mesh):
    placed = (P("sp", "tp"), P("sp"), P(), P(None, "sp", "tp"), P(None, "sp", "tp"), P())
    return jax.shard_map(
        shards, mesh=mesh, in_specs=placed, out_specs=P("sp", "tp"), check_vma=False
    )
```

time: 251 us -> 328 us (1.31)
  the two profiles are of different devices: /device:TPU:256 before, /device:TPU:1 now
where the time goes in v1:
time: 328 us; the launch traced here: 327 us
  waiting for transfers between devices  190 us (58%)
  blocking collectives  59 us (18%)
  starting transfers between devices  35.6 us (11%)
  Pallas kernels  15.5 us (5%)
  between operations  13.9 us (4%)
  local copies, waits for them, and re-layouts  12.8 us (4%)
    all_to_all x3, waiting for transfers between devices, spread(): lax.all_to_all(copies, axis, split_axis=0, concat_axis=0, tiled=True, axi...  156 us
    all_to_all x2, blocking collectives, spread(): lax.all_to_all(copies, axis, split_axis=0, concat_axis=0, tiled=True, axi...  59 us
    all_to_all x3, starting transfers between devices, spread(): lax.all_to_all(copies, axis, split_axis=0, concat_axis=0, tiled=True, axi...  19.4 us
    ppermute x2, waiting for transfers between devices, shards(): other = lax.ppermute(pooled, 'tp', partner)  18.7 us
    pallas_call x2, Pallas kernels, project_pool(): pl.pallas_call(kernel, out_shape=jax.ShapeDtypeStruct((rows - WIN, BLOCK)...  12.5 us
    ppermute x3, waiting for transfers between devices, shards(): lax.ppermute(current, 'tp', tp_perm(lambda t, k=k: t - 2 * k))  10.9 us
    ppermute x3, starting transfers between devices, shards(): lax.ppermute(current, 'tp', tp_perm(lambda t, k=k: t - 2 * k))  8.41 us
  transfers between devices with their start and end apart: 11, of which 9 were waited for; matrix products, arithmetic and copies ran while one was open for 1% of the time, Pallas kernels for 2%

profile of v1, /device:TPU:1, one launch (start us, length us, event | category | flops | bytes accessed | tf_op | source)
XLA Modules:
  0.0 326.8 jit_solution(12124923672696447642)
XLA Ops:
  8.3 18.2 %all_to_all.25 = bf16[8,80,256]{2,1,0:T(8,128)(2,1)S(1)} all-to-all(bf16[8,80,256]{2,1,0:T(8,128)(2,1)S(1)} %broadcast_in_dim.25), channel_id=1, replica_groups={{0,8,16,24,32,40,48,56},{64,72,80,88,96,104,112,120},{128,136,144,152,1..., dimensions={0} | all-to-all | bytes 655360 | tf_op jit(solution)/shard_map/all_to_all | solution.py:40
  27.3 11.0 %all-to-all-start.3 = ((bf16[8,80,256]{2,1,0:T(8,128)(2,1)}), bf16[8,80,256]{2,1,0:T(8,128)(2,1)S(1)}, u32[]{:S(2)}, u32[]{:S(2)}) async-start(bf16[8,80,256]{2,1,0:T(8,128)(2,1)} %broadcast_in_dim.27), calls=%async_computation.3 | async-start | bytes 655360 | tf_op jit(solution)/shard_map/all_to_all | solution.py:40
  41.0 7.8 %all-to-all-done.3 = bf16[8,80,256]{2,1,0:T(8,128)(2,1)S(1)} async-done(((bf16[8,80,256]{2,1,0:T(8,128)(2,1)}), bf16[8,80,256]{2,1,0:T(8,128)(2,1)S(1)}, u32[]{:S(2)}, u32[]{:S(2)}) %all-to-all-start.3) | async-done | bytes 327712 | tf_op jit(solution)/shard_map/all_to_all | solution.py:40
  49.0 40.8 %all_to_all.26.refs_1_ = bf16[8,320,512]{2,1,0:T(8,128)(2,1)} all-to-all(bf16[8,320,512]{2,1,0:T(8,128)(2,1)S(1)} %broadcast_in_dim.23), channel_id=1, replica_groups=mesh['sp'=64,'tp'=8] {'tp'}, dimensions={0} | all-to-all | bytes 5242880 | tf_op jit(solution)/shard_map/all_to_all | solution.py:40
  89.8 1.8 broadcast_in_dim.26
  91.6 3.8 %all-to-all-start.2 = ((bf16[8,640,256]{2,1,0:T(8,128)(2,1)}), bf16[8,640,256]{2,1,0:T(8,128)(2,1)S(1)}, u32[]{:S(2)}, u32[]{:S(2)}) async-start(bf16[8,640,256]{2,1,0:T(8,128)(2,1)} %broadcast_in_dim.26), calls=%async_computation.2 | async-start | bytes 5242880 | tf_op jit(solution)/shard_map/all_to_all | solution.py:40
  96.1 65.3 %all-to-all-done.2 = bf16[8,640,256]{2,1,0:T(8,128)(2,1)S(1)} async-done(((bf16[8,640,256]{2,1,0:T(8,128)(2,1)}), bf16[8,640,256]{2,1,0:T(8,128)(2,1)S(1)}, u32[]{:S(2)}, u32[]{:S(2)}) %all-to-all-start.2) | async-done | bytes 2621472 | tf_op jit(solution)/shard_map/all_to_all | solution.py:40
  161.4 1.7 broadcast_in_dim.28
  163.1 4.6 %all-to-all-start.4 = ((bf16[8,640,256]{2,1,0:T(8,128)(2,1)}), bf16[8,640,256]{2,1,0:T(8,128)(2,1)}, u32[]{:S(2)}, u32[]{:S(2)}) async-start(bf16[8,640,256]{2,1,0:T(8,128)(2,1)} %broadcast_in_dim.28), calls=%async_computation.4 | async-start | bytes 5242880 | tf_op jit(solution)/shard_map/all_to_all | solution.py:40
  168.3 83.4 %all-to-all-done.4 = bf16[8,640,256]{2,1,0:T(8,128)(2,1)} async-done(((bf16[8,640,256]{2,1,0:T(8,128)(2,1)}), bf16[8,640,256]{2,1,0:T(8,128)(2,1)}, u32[]{:S(2)}, u32[]{:S(2)}) %all-to-all-start.4) | async-done | bytes 2621472 | tf_op jit(solution)/shard_map/all_to_all | solution.py:40
  253.7 6.1 %project_pool.2.refs_1_ = bf16[304,512]{1,0:T(8,128)(2,1)S(1)} custom-call(s32[8]{0:T(128)S(1)} %iota.7.refs_0_, bf16[8,320,512]{2,1,0:T(8,128)(2,1)S(1)} %copy-done.1, f32[8,512]{1,0:T(8,128)S(1)} %squeeze.18.refs_2_, f32[5,320,128]{2,1,0:T(8,128)S(1)} %broadcast_in_dim.24.refs_3_, bf16[8,8,80,256]{3,2,1,0:T(8,128)(2,1)S(1)} %bitcast.16, ...), custom_call_target="tpu_custom_call" | custom-call | flops 1342177280 | bytes 7340032 | tf_op jit(solution)/shard_map/project_pool/pallas_call | solution.py:107
  259.8 1.9 collective-permute-start.1
  262.6 9.0 %collective-permute-done.1.refs_2_ = bf16[304,512]{1,0:T(8,128)(2,1)S(1)} collective-permute-done((bf16[304,512]{1,0:T(8,128)(2,1)S(1)}, bf16[304,512]{1,0:T(8,128)(2,1)S(1)}, u32[]{:S(2)}, u32[]{:S(2)}) %collective-permute-start.1) | collective-permute-done | bytes 311328 | tf_op jit(solution)/shard_map/ppermute | solution.py:220
  273.3 1.9 collective-permute-start.3
  275.3 1.9 collective-permute-start.4
  277.2 4.6 %collective-permute-start.2 = (bf16[304,512]{1,0:T(8,128)(2,1)S(1)}, bf16[304,512]{1,0:T(8,128)(2,1)S(1)}, u32[]{:S(2)}, u32[]{:S(2)}) collective-permute-start(bf16[304,512]{1,0:T(8,128)(2,1)S(1)} %mix.2), channel_id=1, source_target_pairs={{0,6},{1,7},{2,0},{3,1},{4,2},{5,3},{6,4},{7,5},{8,14},{9,15},{10,... | collective-permute-start | bytes 933896 | tf_op jit(solution)/shard_map/ppermute | solution.py:223
  281.8 2.6 collective-permute-done.3
  284.4 8.3 %collective-permute-done.4 = bf16[304,512]{1,0:T(8,128)(2,1)S(1)} collective-permute-done((bf16[304,512]{1,0:T(8,128)(2,1)S(1)}, bf16[304,512]{1,0:T(8,128)(2,1)S(1)}, u32[]{:S(2)}, u32[]{:S(2)}) %collective-permute-start.4) | collective-permute-done | bytes 311328 | tf_op jit(solution)/shard_map/ppermute | solution.py:223
  292.9 2.4 collective-permute-start.5
  295.5 2.3 collective-permute-done.5.refs_2_
  298.1 2.5 copy-done
  300.6 6.4 %project_pool.3.refs_1_ = bf16[288,512]{1,0:T(8,128)(2,1)S(1)} custom-call(s32[8]{0:T(128)S(1)} %pad_add_fusion.refs_0_, bf16[4,304,512]{2,1,0:T(8,128)(2,1)S(1)} %pad_maximum_fusion.refs_1_, bf16[4,304,512]{2,1,0:T(8,128)(2,1)S(1)} %collective-permute-done.5.refs_2_, f32[8,512]{1,0:T(8,128)S(1)} %squeeze.22.refs_3_, ...), custom_call_target="tpu_custom_call" | custom-call | flops 1275068416 | bytes 7340032 | tf_op jit(solution)/shard_map/project_pool/pallas_call | solution.py:107
  307.0 1.9 collective-permute-start.6
  308.9 9.7 %collective-permute-done.6.refs_2_ = bf16[288,512]{1,0:T(8,128)(2,1)S(1)} collective-permute-done((bf16[288,512]{1,0:T(8,128)(2,1)S(1)}, bf16[288,512]{1,0:T(8,128)(2,1)S(1)}, u32[]{:S(2)}, u32[]{:S(2)}) %collective-permute-start.6) | collective-permute-done | bytes 294944 | tf_op jit(solution)/shard_map/ppermute | solution.py:229
  (68 shorter events, 12.9 us)
Async XLA Ops:
  6.5 31.8 %copy-start.4 = (s32[288]{0:T(512)S(1)}, s32[288]{0:T(512)}, u32[]{:S(2)}) copy-start(s32[288]{0:T(512)} %param.7) | copy-start | bytes 3460
  6.5 31.8 %slice-start = ((bf16[288,512]{1,0:T(8,128)(2,1)}), bf16[32,512]{1,0:T(8,128)(2,1)S(1)}, s32[]{:S(2)}) async-start(bf16[288,512]{1,0:T(8,128)(2,1)} %param.6), calls=%async_computation.6 | async-start | bytes 65536 | tf_op jit(solution)/shard_map/slice | solution.py:194
  7.5 33.5 %copy-start.2 = (bf16[288,512]{1,0:T(8,128)(2,1)S(1)}, bf16[288,512]{1,0:T(8,128)(2,1)}, u32[]{:S(2)}) copy-start(bf16[288,512]{1,0:T(8,128)(2,1)} %param.6) | copy-start | bytes 884740
  27.3 21.5 %all-to-all-start.3 = ((bf16[8,80,256]{2,1,0:T(8,128)(2,1)}), bf16[8,80,256]{2,1,0:T(8,128)(2,1)S(1)}, u32[]{:S(2)}, u32[]{:S(2)}) async-start(bf16[8,80,256]{2,1,0:T(8,128)(2,1)} %broadcast_in_dim.27), calls=%async_computation.3 | async-start | bytes 655360 | tf_op jit(solution)/shard_map/all_to_all | solution.py:40
  38.4 2.6 collective-permute-start
  91.6 69.8 %all-to-all-start.2 = ((bf16[8,640,256]{2,1,0:T(8,128)(2,1)}), bf16[8,640,256]{2,1,0:T(8,128)(2,1)S(1)}, u32[]{:S(2)}, u32[]{:S(2)}) async-start(bf16[8,640,256]{2,1,0:T(8,128)(2,1)} %broadcast_in_dim.26), calls=%async_computation.2 | async-start | bytes 5242880 | tf_op jit(solution)/shard_map/all_to_all | solution.py:40
  95.4 202.4 %all-gather.3.cloned.1.call-start = ((), (), s32[]{:S(2)}) async-start(), calls=%async_computation.5 | async-start | bytes 5324800 | tf_op jit(solution)/shard_map/all_gather | solution.py:180
  163.1 4.6 %copy-start.3 = (f32[2,4096]{1,0:T(2,128)S(1)}, f32[2,4096]{1,0:T(2,128)}, u32[]{:S(2)}) copy-start(f32[2,4096]{1,0:T(2,128)} %param.8) | copy-start | bytes 98308
  163.1 88.6 %all-to-all-start.4 = ((bf16[8,640,256]{2,1,0:T(8,128)(2,1)}), bf16[8,640,256]{2,1,0:T(8,128)(2,1)}, u32[]{:S(2)}, u32[]{:S(2)}) async-start(bf16[8,640,256]{2,1,0:T(8,128)(2,1)} %broadcast_in_dim.28), calls=%async_computation.4 | async-start | bytes 5242880 | tf_op jit(solution)/shard_map/all_to_all | solution.py:40
  252.0 1.7 copy-start.1
  259.8 11.8 %collective-permute-start.1 = (bf16[304,512]{1,0:T(8,128)(2,1)S(1)}, bf16[304,512]{1,0:T(8,128)(2,1)S(1)}, u32[]{:S(2)}, u32[]{:S(2)}) collective-permute-start(bf16[304,512]{1,0:T(8,128)(2,1)S(1)} %project_pool.2.refs_1_), channel_id=1, source_target_pairs={{0,4},{1,5},{2,6},{3,7},{4,0},{5,1},{6,2},{7,3},{8,12},{9,13},{10,... | collective-permute-start | bytes 933896 | tf_op jit(solution)/shard_map/ppermute | solution.py:220
  273.3 11.0 %collective-permute-start.3 = (bf16[304,512]{1,0:T(8,128)(2,1)S(1)}, bf16[304,512]{1,0:T(8,128)(2,1)S(1)}, u32[]{:S(2)}, u32[]{:S(2)}) collective-permute-start(bf16[304,512]{1,0:T(8,128)(2,1)S(1)} %mix.2), channel_id=1, source_target_pairs={{0,4},{1,5},{2,6},{3,7},{4,0},{5,1},{6,2},{7,3},{8,12},{9,13},{10,... | collective-permute-start | bytes 933896 | tf_op jit(solution)/shard_map/ppermute | solution.py:223
  275.3 17.4 %collective-permute-start.4 = (bf16[304,512]{1,0:T(8,128)(2,1)S(1)}, bf16[304,512]{1,0:T(8,128)(2,1)S(1)}, u32[]{:S(2)}, u32[]{:S(2)}) collective-permute-start(bf16[304,512]{1,0:T(8,128)(2,1)S(1)} %mix.2), channel_id=1, source_target_pairs={{0,2},{1,3},{2,4},{3,5},{4,6},{5,7},{6,0},{7,1},{8,10},{9,11},{10,... | collective-permute-start | bytes 933896 | tf_op jit(solution)/shard_map/ppermute | solution.py:223
  277.2 15.5 %collective-permute-start.2 = (bf16[304,512]{1,0:T(8,128)(2,1)S(1)}, bf16[304,512]{1,0:T(8,128)(2,1)S(1)}, u32[]{:S(2)}, u32[]{:S(2)}) collective-permute-start(bf16[304,512]{1,0:T(8,128)(2,1)S(1)} %mix.2), channel_id=1, source_target_pairs={{0,6},{1,7},{2,0},{3,1},{4,2},{5,3},{6,4},{7,5},{8,14},{9,15},{10,... | collective-permute-start | bytes 933896 | tf_op jit(solution)/shard_map/ppermute | solution.py:223
  292.9 5.0 %collective-permute-start.5 = (bf16[4,304,512]{2,1,0:T(8,128)(2,1)S(1)}, bf16[4,304,512]{2,1,0:T(8,128)(2,1)S(1)}, u32[]{:S(2)}, u32[]{:S(2)}) collective-permute-start(bf16[4,304,512]{2,1,0:T(8,128)(2,1)S(1)} %pad_maximum_fusion.refs_1_), channel_id=1, source_target_pairs={{0,1},{1,0},{2,3},{3,2},{4,5},{5,4},{6,7},{7,6},{8,9},{9,8},{10,11... | collective-permute-start | bytes 3735560 | tf_op jit(solution)/shard_map/ppermute | solution.py:225
  298.1 2.5 copy-start
  307.0 11.6 %collective-permute-start.6 = (bf16[288,512]{1,0:T(8,128)(2,1)S(1)}, bf16[288,512]{1,0:T(8,128)(2,1)S(1)}, u32[]{:S(2)}, u32[]{:S(2)}) collective-permute-start(bf16[288,512]{1,0:T(8,128)(2,1)S(1)} %project_pool.3.refs_1_), channel_id=1, source_target_pairs={{0,4},{1,5},{2,6},{3,7},{4,0},{5,1},{6,2},{7,3},{8,12},{9,13},{10,... | collective-permute-start | bytes 884744 | tf_op jit(solution)/shard_map/ppermute | solution.py:229
Sparse Core Ops, SparseCore 0:
  99.2 143.6 all-gather.2
